TPU v7x, 32 devices: a whole 2x2x4 slice. The times are simulated.
32 devices in a mesh: ep: 8 (over z, x), tp: 4 (over y, core).
Axes of the slice: x: 2, y: 2, z: 4, core: 2. Of those that a mesh axis runs over, the one named last changes fastest.
Arguments:
- tokens: bfloat16 [1024, 2048], P('ep'), may hold values from -6 to 6
- cotangent: bfloat16 [1024, 2048], P('ep'), may hold values from -1.5 to 1.5
- routes: int32 [1024, 2], P('ep'), may hold values from 0 to 3, all different within a row; in each aligned block of 128 rows (0 to 127, 128 to 255, ...) at most 96 rows name the same one
- router: bfloat16 [2048, 4], replicated, may hold values from -0.125 to 0.125
- w_gate: bfloat16 [8, 2048, 2048], P('ep', None, 'tp'), may hold values from -0.125 to 0.125
- w_up: bfloat16 [8, 2048, 2048], P('ep', None, 'tp'), may hold values from -0.125 to 0.125
- w_down: bfloat16 [8, 2048, 2048], P('ep', 'tp'), may hold values from -0.09375 to 0.09375
Outputs:
- token_grad: bfloat16 [1024, 2048], P('ep', 'tp')
- gate_grad: float32 [1024, 2], P('ep')
- grad_gate: bfloat16 [8, 2048, 2048], P('ep', None, 'tp')
- grad_up: bfloat16 [8, 2048, 2048], P('ep', None, 'tp')
- grad_down: bfloat16 [8, 2048, 2048], P('ep', 'tp')
- router_grad: float32 [2048, 4], P(('ep', 'tp'))
Inputs may be any that keep to these rules, and one draw needn't show every extreme that they name: `routes`: each row names 2 different experts. In the rows of one index of ep (aligned blocks of 128 rows) no expert is named by more than 96 rows, a bound that some block reaches.
All inputs are finite; a program needn't handle non-finite values.
Results may differ from a plain program's by a relative error of at most 0.018.
Values may be sent and summed in bfloat16 or wider, within the bound.
A program may use at most 64 MiB of HBM per device.

v0:
```python
import jax
import jax.numpy as jnp
from jax import lax
from jax.sharding import PartitionSpec as P

BLOCKS = 2


def build_slots(block_routes, experts, capacity):
    flat_routes = block_routes.reshape(-1)
    labels = jnp.arange(experts, dtype=jnp.int32)
    hit_mask = (flat_routes[None, :] == labels[:, None]).astype(jnp.int32)
    rank_in = jnp.cumsum(hit_mask, axis=1, dtype=jnp.int32) - 1
    slot_ids = jnp.arange(capacity, dtype=jnp.int32)
    assigned = (hit_mask[:, None, :] == 1) & (rank_in[:, None, :] == slot_ids[None, :, None])
    return assigned.astype(jnp.float32)


def gate_pair(tokens, routes, router, experts):
    logits = jnp.dot(tokens, router, preferred_element_type=jnp.float32)
    labels = jnp.arange(experts, dtype=jnp.int32)
    picked = (routes[:, :, None] == labels[None, None, :]).astype(jnp.float32)
    chosen = jnp.sum(picked * logits[:, None, :], axis=2)
    margin = chosen[:, 0] - chosen[:, 1]
    weights = jnp.stack([jax.nn.sigmoid(margin), jax.nn.sigmoid(-margin)], axis=1)
    return (picked, weights)


def logit_grads(picked, weights, gate_grad):
    lead_grad = weights[:, 0] * weights[:, 1] * (gate_grad[:, 0] - gate_grad[:, 1])
    pair_grad = jnp.stack([lead_grad, -lead_grad], axis=1)
    return jnp.sum(picked * pair_grad[:, :, None], axis=1)


def expert_grads(rows_in, cot_in, gate_in, gate_weight, up_weight, down_weight):
    pre_gate = jnp.dot(rows_in, gate_weight, preferred_element_type=jnp.float32)
    pre_up = jnp.dot(rows_in, up_weight, preferred_element_type=jnp.float32)
    back_grad = lax.dot_general(
        cot_in, down_weight, (((1,), (1,)), ((), ())), preferred_element_type=jnp.float32
    )
    sig_gate = jax.nn.sigmoid(pre_gate)
    active = pre_gate * sig_gate
    hidden = (active * pre_up).astype(jnp.bfloat16)
    gate_terms = jnp.sum(hidden.astype(jnp.float32) * back_grad, axis=1)
    gate_col = gate_in.astype(jnp.float32)[:, None]
    scaled_back = gate_col * back_grad
    d_gate = (scaled_back * pre_up * sig_gate * (1.0 + pre_gate * (1.0 - sig_gate))).astype(
        jnp.bfloat16
    )
    d_up = (scaled_back * active).astype(jnp.bfloat16)
    scaled_cot = (gate_col * cot_in.astype(jnp.float32)).astype(jnp.bfloat16)
    contract_rows = (((0,), (0,)), ((), ()))
    grad_gate = lax.dot_general(
        rows_in, d_gate, contract_rows, preferred_element_type=jnp.float32
    ).astype(jnp.bfloat16)
    grad_up = lax.dot_general(
        rows_in, d_up, contract_rows, preferred_element_type=jnp.float32
    ).astype(jnp.bfloat16)
    grad_down = lax.dot_general(
        hidden, scaled_cot, contract_rows, preferred_element_type=jnp.float32
    ).astype(jnp.bfloat16)
    return (d_gate, d_up, gate_terms, grad_gate, grad_up, grad_down)


def spread_slabs(packed, experts, slab_count):
    widened = jnp.broadcast_to(packed[:, None], (experts, BLOCKS) + packed.shape[1:])
    return widened.reshape((slab_count,) + packed.shape[1:])


def shards(tokens, cotangent, routes, router, w_gate, w_up, w_down):
    highest = lax.Precision.HIGHEST
    ep_count = lax.axis_size("ep")
    tp_count = lax.axis_size("tp")
    experts = ep_count // BLOCKS
    tok_rows, width = tokens.shape
    top_count = routes.shape[1]
    capacity = 3 * tok_rows * top_count // (2 * experts)
    col_width = width // tp_count
    tp_index = lax.axis_index("tp")
    picked, weights = gate_pair(tokens, routes, router, experts)
    assigned = build_slots(routes, experts, capacity)
    per_token = jnp.sum(assigned.reshape(experts, capacity, tok_rows, top_count), axis=3)
    token_map = per_token.astype(jnp.bfloat16)
    gate_send = weights.astype(jnp.bfloat16)
    gate_slots = jnp.einsum(
        "ecj,j->ec", assigned, gate_send.astype(jnp.float32).reshape(-1), precision=highest
    ).astype(jnp.bfloat16)
    gate_out = spread_slabs(gate_slots, experts, ep_count)

    def pack_rows(source):
        packed = jnp.einsum(
            "ect,td->ecd", token_map, source, preferred_element_type=jnp.float32
        ).astype(jnp.bfloat16)
        return spread_slabs(packed, experts, ep_count)

    tok_part = lax.dynamic_slice_in_dim(tokens, tp_index * col_width, col_width, 1)
    cot_part = lax.dynamic_slice_in_dim(cotangent, tp_index * col_width, col_width, 1)
    recv_part, recv_cot_part, recv_gate = (
        lax.all_to_all(pack_rows(tok_part), "ep", split_axis=0, concat_axis=0, tiled=True),
        lax.all_to_all(pack_rows(cot_part), "ep", split_axis=0, concat_axis=0, tiled=True),
        lax.all_to_all(gate_out, "ep", split_axis=0, concat_axis=0, tiled=True),
    )
    recv_rows, recv_cot = (
        lax.all_gather(recv_part, "tp", axis=2, tiled=True),
        lax.all_gather(recv_cot_part, "tp", axis=2, tiled=True),
    )
    rows_in = recv_rows.reshape(-1, width)
    cot_in = recv_cot.reshape(-1, width)
    gate_in = recv_gate.reshape(-1)
    d_gate, d_up, gate_terms, grad_gate, grad_up, grad_down = expert_grads(
        rows_in, cot_in, gate_in, w_gate[0], w_up[0], w_down[0]
    )
    contract_hidden = (((1,), (1,)), ((), ()))
    partial_dx = lax.dot_general(
        d_gate, w_gate[0], contract_hidden, preferred_element_type=jnp.float32
    )
    partial_dx = partial_dx + lax.dot_general(
        d_up, w_up[0], contract_hidden, preferred_element_type=jnp.float32
    )
    summed_dx = lax.psum_scatter(
        partial_dx.reshape(ep_count, capacity, width).astype(jnp.bfloat16),
        "tp",
        scatter_dimension=2,
        tiled=True,
    ).astype(jnp.float32)
    gate_sums = lax.psum(gate_terms.reshape(ep_count, capacity), "tp")
    back_dx, back_gate = (
        lax.all_to_all(
            summed_dx.astype(jnp.bfloat16), "ep", split_axis=0, concat_axis=0, tiled=True
        ).astype(summed_dx.dtype),
        lax.all_to_all(
            gate_sums.astype(jnp.bfloat16), "ep", split_axis=0, concat_axis=0, tiled=True
        ).astype(gate_sums.dtype),
    )
    slab_dx = jnp.sum(back_dx.reshape(experts, BLOCKS, capacity, col_width), axis=1)
    routed_dx = jnp.einsum("ect,ecd->td", per_token, slab_dx, precision=highest)
    slab_gate = jnp.sum(back_gate.reshape(experts, BLOCKS, capacity), axis=1)
    gate_grad = jnp.einsum("ecj,ec->j", assigned, slab_gate, precision=highest).reshape(
        tok_rows, top_count
    )
    logit_grad = logit_grads(picked, weights, gate_grad)
    router_cols = lax.dynamic_slice_in_dim(router, tp_index * col_width, col_width, 0).astype(
        jnp.float32
    )
    token_grad = (routed_dx + jnp.dot(logit_grad, router_cols.T, precision=highest)).astype(
        jnp.bfloat16
    )
    seg_rows = tok_rows // tp_count
    own_rows = lax.dynamic_slice_in_dim(tokens, tp_index * seg_rows, seg_rows, 0).astype(
        jnp.float32
    )
    own_logit = lax.dynamic_slice_in_dim(logit_grad, tp_index * seg_rows, seg_rows, 0)
    router_grad = lax.psum_scatter(
        jnp.dot(own_rows.T, own_logit, precision=highest),
        ("ep", "tp"),
        scatter_dimension=0,
        tiled=True,
    )
    return (token_grad, gate_grad, grad_gate[None], grad_up[None], grad_down[None], router_grad)


def solution(mesh):
    placed = (
        P("ep", None),
        P("ep", None),
        P("ep", None),
        P(),
        P("ep", None, "tp"),
        P("ep", None, "tp"),
        P("ep", "tp", None),
    )
    return jax.shard_map(
        shards,
        mesh=mesh,
        in_specs=placed,
        out_specs=(
            P("ep", "tp"),
            P("ep", None),
            P("ep", None, "tp"),
            P("ep", None, "tp"),
            P("ep", "tp", None),
            P(("ep", "tp"), None),
        ),
        check_vma=False,
    )
```

profile of v0, /device:TPU:0, one launch (start us, length us, event | category | flops | bytes accessed | tf_op | source)
XLA Modules:
  0.0 325.1 jit_solution(1084350082928045645)
XLA Ops:
  8.3 1.2 reduce-window.6
  12.1 27.3 %all_to_all.33 = bf16[8,96,512]{2,1,0:T(8,128)(2,1)} all-to-all(bf16[8,96,512]{2,1,0:T(8,128)(2,1)S(1)} %bitcast.80), channel_id=1, replica_groups=mesh['ep'=8,'tp'=4] {'ep'}, dimensions={0} | all-to-all | bytes 1572864 | tf_op jit(solution)/shard_map/all_to_all | solution.py:99
  39.5 1.2 convolution_convert_fusion.3
  40.8 23.3 %all_to_all.34 = bf16[8,96,512]{2,1,0:T(8,128)(2,1)} all-to-all(bf16[8,96,512]{2,1,0:T(8,128)(2,1)S(1)} %bitcast.81), channel_id=1, replica_groups=mesh['ep'=8,'tp'=4] {'ep'}, dimensions={0} | all-to-all | bytes 1572864 | tf_op jit(solution)/shard_map/all_to_all | solution.py:100
  64.7 2.4 all-gather.5.cloned.1.call-done
  67.1 5.7 %fusion.11 = f32[768,512]{0,1:T(8,128)} fusion(bf16[768,2048]{1,0:T(8,128)(2,1)} %bitcast.95, bf16[1,2048,512]{2,1,0:T(8,128)(2,1)} %param.12), kind=kOutput, calls=%fused_computation.15 | convolution fusion | flops 1610612736 | bytes 6815744 | tf_op jit(solution)/shard_map/dot_general | solution.py:37
  72.8 3.0 fusion.8
  75.8 21.4 %all-gather.3.cloned.1.call-done = bf16[8,96,2048]{2,1,0:T(8,128)(2,1)} async-done(((bf16[8,96,512]{2,1,0:T(8,128)(2,1)}), bf16[8,96,2048]{2,1,0:T(8,128)(2,1)}) %all-gather.3.cloned.1.call-update) | async-done | bytes 3145744 | tf_op jit(solution)/shard_map/all_gather | solution.py:105
  97.2 6.7 %multiply_reduce_fusion = (f32[768]{0:T(1024)S(1)}, bf16[768,512]{0,1:T(8,128)(2,1)}, f32[768,512]{0,1:T(8,128)}) fusion(f32[768,512]{0,1:T(8,128)} %fusion.11, f32[768,512]{0,1:T(8,128)} %fusion.8, bf16[768,2048]{1,0:T(8,128)(2,1)} %bitcast.99, bf16[1,512,2048]{2,1,0:T(8,128)(2,1)} %param.13), kind=kOutput, calls=%fused_computation.20 | convolution fusion | flops 1614150912 | bytes 10750976 | tf_op jit(solution)/shard_map/dot_general | solution.py:38
  104.1 5.9 %psum.7 = bf16[8,96]{1,0:T(8,128)(2,1)S(1)} all-reduce(f32[8,96]{1,0:T(8,128)S(1)} %reshape.150), channel_id=1, replica_groups=mesh['ep'=8,'tp'=4] {'tp'}, use_global_device_ids=true, to_apply=%region_7.8 | all-reduce | flops 768 | bytes 4608 | tf_op jit(solution)/shard_map/psum | solution.py:126
  110.5 5.7 %all-to-all-start.4 = ((bf16[8,1,96]{2,1,0:T(2,128)(2,1)}), bf16[8,1,96]{2,1,0:T(2,128)(2,1)S(1)}, u32[]{:S(2)}, u32[]{:S(2)}) async-start(bf16[8,1,96]{2,1,0:T(2,128)(2,1)} %copy.80), calls=%async_computation.5 | async-start | bytes 8192 | tf_op jit(solution)/shard_map/all_to_all | solution.py:131
  116.5 6.1 %all-to-all-done.4 = bf16[8,1,96]{2,1,0:T(2,128)(2,1)S(1)} async-done(((bf16[8,1,96]{2,1,0:T(2,128)(2,1)}), bf16[8,1,96]{2,1,0:T(2,128)(2,1)S(1)}, u32[]{:S(2)}, u32[]{:S(2)}) %all-to-all-start.4) | async-done | bytes 1568 | tf_op jit(solution)/shard_map/all_to_all | solution.py:131
  123.4 8.9 %all_to_all.35 = bf16[8,1,96]{2,1,0:T(2,128)(2,1)S(1)} all-to-all(bf16[8,1,96]{2,1,0:T(2,128)(2,1)S(1)} %copy.77), channel_id=1, replica_groups=mesh['ep'=8,'tp'=4] {'ep'}, dimensions={0} | all-to-all | bytes 3072 | tf_op jit(solution)/shard_map/all_to_all | solution.py:101
  132.4 3.1 multiply_convert_fusion.7
  135.5 1.8 fusion.6
  137.7 3.5 %add_convert_fusion = bf16[768,2048]{1,0:T(8,128)(2,1)} fusion(f32[768,2048]{1,0:T(8,128)S(1)} %fusion.6, bf16[768,512]{0,1:T(8,128)(2,1)S(1)} %get-tuple-element.12, bf16[1,2048,512]{2,1,0:T(8,128)(2,1)S(1)} %copy-done.4), kind=kOutput, calls=%fused_computation.1 | convolution fusion | flops 1613758464 | bytes 12320768 | tf_op jit(solution)/shard_map/dot_general | solution.py:117
  141.4 1.8 fusion.31
  143.2 33.2 %reduce-scatter.5.cloned.1.call-done = bf16[8,96,512]{2,1,0:T(8,128)(2,1)} async-done(((bf16[8,96,2048]{2,1,0:T(8,128)(2,1)}), bf16[8,96,512]{2,1,0:T(8,128)(2,1)}) %reduce-scatter.5.cloned.1.call-update) | async-done | bytes 786448 | tf_op jit(solution)/shard_map/reduce_scatter | solution.py:120
  176.4 5.5 %all-to-all-start.3 = ((bf16[8,96,512]{2,1,0:T(8,128)(2,1)}), bf16[8,96,512]{2,1,0:T(8,128)(2,1)S(1)}, u32[]{:S(2)}, u32[]{:S(2)}) async-start(bf16[8,96,512]{2,1,0:T(8,128)(2,1)} %reduce-scatter.5.cloned.1.call-done), calls=%async_computation.4 | async-start | bytes 1572864 | tf_op jit(solution)/shard_map/all_to_all | solution.py:128
  181.9 5.4 %fusion.3 = bf16[1,2048,512]{2,1,0:T(8,128)(2,1)} fusion(bf16[768,2048]{1,0:T(8,128)(2,1)} %bitcast.96, bf16[768,512]{0,1:T(8,128)(2,1)} %copy-done.3), kind=kOutput, calls=%fused_computation.7 | convolution fusion | flops 1611661312 | bytes 6029312 | tf_op jit(solution)/shard_map/dot_general | solution.py:53
  187.3 3.2 fusion.5
  190.6 3.2 fusion.4
  193.8 121.5 %reduce-scatter.7.cloned.1.call-done = f32[64,4]{1,0:T(8,128)} async-done(((f32[2048,4]{1,0:T(8,128)}), f32[64,4]{1,0:T(8,128)}) %reduce-scatter.7.cloned.1.call-update) | async-done | bytes 1040
  315.3 1.4 copy.85
  (81 shorter events, 8.4 us)
Async XLA Ops:
  7.2 65.6 %copy-start = (bf16[1,2048,512]{2,1,0:T(8,128)(2,1)S(1)}, bf16[1,2048,512]{2,1,0:T(8,128)(2,1)}, u32[]{:S(2)}) copy-start(bf16[1,2048,512]{2,1,0:T(8,128)(2,1)} %param.11) | copy-start | bytes 6291460
  7.2 60.0 %all-gather.5.cloned.1.call-start = ((), (), s32[]{:S(2)}) async-start(), calls=%async_computation.8 | async-start | bytes 3932160 | tf_op jit(solution)/shard_map/all_gather | solution.py:104
  39.4 24.9 %copy-start.7 = (s32[128,2]{0,1:T(2,128)S(1)}, s32[128,2]{0,1:T(2,128)}, u32[]{:S(2)}) copy-start(s32[128,2]{0,1:T(2,128)} %param.9) | copy-start | bytes 3076
  39.5 25.0 %copy-start.5 = (bf16[128,2048]{1,0:T(8,128)(2,1)S(1)}, bf16[128,2048]{1,0:T(8,128)(2,1)}, u32[]{:S(2)}) copy-start(bf16[128,2048]{1,0:T(8,128)(2,1)} %param.7) | copy-start | bytes 1572868
  39.5 25.0 %copy-start.6 = (bf16[2048,4]{0,1:T(4,128)(2,1)S(1)}, bf16[2048,4]{0,1:T(4,128)(2,1)}, u32[]{:S(2)}) copy-start(bf16[2048,4]{0,1:T(4,128)(2,1)} %param.10) | copy-start | bytes 49156
  39.5 57.8 %all-gather.3.cloned.1.call-start = ((), (), s32[]{:S(2)}) async-start(), calls=%async_computation.7 | async-start | bytes 3932160 | tf_op jit(solution)/shard_map/all_gather | solution.py:105
  67.1 5.7 %copy-start.9 = (bf16[8,96,2048]{2,1,0:T(8,128)(2,1)S(1)}, bf16[8,96,2048]{2,1,0:T(8,128)(2,1)}, u32[]{:S(2)}) copy-start(bf16[8,96,2048]{2,1,0:T(8,128)(2,1)} %all-gather.5.cloned.1.call-done) | copy-start | bytes 9437188
  110.5 12.1 %all-to-all-start.4 = ((bf16[8,1,96]{2,1,0:T(2,128)(2,1)}), bf16[8,1,96]{2,1,0:T(2,128)(2,1)S(1)}, u32[]{:S(2)}, u32[]{:S(2)}) async-start(bf16[8,1,96]{2,1,0:T(2,128)(2,1)} %copy.80), calls=%async_computation.5 | async-start | bytes 8192 | tf_op jit(solution)/shard_map/all_to_all | solution.py:131
  116.2 60.2 %reduce-scatter.5.cloned.1.call-start = ((), (), s32[]{:S(2)}) async-start(), calls=%async_computation.9 | async-start | bytes 3932160 | tf_op jit(solution)/shard_map/reduce_scatter | solution.py:120
  122.8 12.7 %copy-start.8 = (f32[1,128,2,1]{1,0,3,2:T(1,128)}, f32[1,128,2,1]{1,0,3,2:T(1,128)S(1)}, u32[]{:S(2)}) copy-start(f32[1,128,2,1]{1,0,3,2:T(1,128)S(1)} %fusion.23) | copy-start | bytes 3076
  135.5 1.9 copy-start.3
  135.5 1.9 copy-start.1
  135.5 2.2 copy-start.4
  141.3 174.1 %reduce-scatter.7.cloned.1.call-start = ((), (), s32[]{:S(2)}) async-start(), calls=%async_computation.10 | async-start | bytes 1081344
  176.4 140.3 %all-to-all-start.3 = ((bf16[8,96,512]{2,1,0:T(8,128)(2,1)}), bf16[8,96,512]{2,1,0:T(8,128)(2,1)S(1)}, u32[]{:S(2)}, u32[]{:S(2)}) async-start(bf16[8,96,512]{2,1,0:T(8,128)(2,1)} %reduce-scatter.5.cloned.1.call-done), calls=%async_computation.4 | async-start | bytes 1572864 | tf_op jit(solution)/shard_map/all_to_all | solution.py:128
  181.9 5.4 %copy-start.11 = (bf16[8,96,2048]{2,1,0:T(8,128)(2,1)S(1)}, bf16[8,96,2048]{2,1,0:T(8,128)(2,1)}, u32[]{:S(2)}) copy-start(bf16[8,96,2048]{2,1,0:T(8,128)(2,1)} %all-gather.3.cloned.1.call-done) | copy-start | bytes 9437188
  181.9 5.4 %copy-start.12 = (bf16[768,512]{0,1:T(8,128)(2,1)S(1)}, bf16[768,512]{0,1:T(8,128)(2,1)}, u32[]{:S(2)}) copy-start(bf16[768,512]{0,1:T(8,128)(2,1)} %get-tuple-element.11) | copy-start | bytes 2359300
  187.3 3.3 %copy-start.2 = (bf16[768,512]{0,1:T(8,128)(2,1)S(1)}, bf16[768,512]{0,1:T(8,128)(2,1)}, u32[]{:S(2)}) copy-start(bf16[768,512]{0,1:T(8,128)(2,1)} %copy-done.1) | copy-start | bytes 2359300
  187.3 3.3 %copy-start.10 = (bf16[8,96,2048]{2,1,0:T(8,128)(2,1)S(1)}, bf16[8,96,2048]{2,1,0:T(8,128)(2,1)}, u32[]{:S(2)}) copy-start(bf16[8,96,2048]{2,1,0:T(8,128)(2,1)} %all-gather.5.cloned.1.call-done) | copy-start | bytes 9437188
Sparse Core Ops, SparseCore 0:
  39.6 27.5 all-gather.4
  68.7 28.4 all-gather.2
  141.4 34.9 reduce-scatter.4
  178.5 136.7 reduce-scatter.6
where the time goes:
time: 326 us; the launch traced here: 325 us
  waiting for transfers between devices  185 us (57%)
  blocking collectives  65.4 us (20%)
  matrix products  39.1 us (12%)
  between operations  14 us (4%)
  starting transfers between devices  11.3 us (3%)
  other arithmetic  5.65 us (2%)
  local copies, waits for them, and re-layouts  4.82 us (1%)
    unnamed x5, waiting for transfers between devices  122 us
    reduce_scatter x1, waiting for transfers between devices, shards(): lax.psum_scatter(partial_dx.reshape(ep_count, capacity, width).astype(jnp...  33.2 us
    all_to_all x1, blocking collectives, shards(): lax.all_to_all(pack_rows(tok_part), 'ep', split_axis=0, concat_axis=0, ti...  27.3 us
    all_to_all x1, blocking collectives, shards(): lax.all_to_all(pack_rows(cot_part), 'ep', split_axis=0, concat_axis=0, ti...  23.3 us
    all_gather x1, waiting for transfers between devices, shards(): lax.all_gather(recv_cot_part, 'tp', axis=2, tiled=True)  21.4 us
    all_to_all x1, blocking collectives, shards(): lax.all_to_all(gate_out, 'ep', split_axis=0, concat_axis=0, tiled=True)  8.86 us
    dot_general x1, matrix products, expert_grads(): lax.dot_general(cot_in, down_weight, (((1,), (1,)), ((), ())), preferred_...  6.74 us
  transfers between devices with their start and end apart: 6, of which 5 were waited for; matrix products, arithmetic and copies ran while one was open for 8% of the time, Pallas kernels for 0%

commit v1 on v0

--- a/solution.py
+++ b/solution.py
@@ -67,7 +67,7 @@
     return widened.reshape((slab_count,) + packed.shape[1:])
 
 
-def shards(tokens, cotangent, routes, router, w_gate, w_up, w_down):
+def routed_shards(tokens, cotangent, routes, router, w_gate, w_up, w_down):
     highest = lax.Precision.HIGHEST
     ep_count = lax.axis_size("ep")
     tp_count = lax.axis_size("tp")
@@ -159,6 +159,117 @@
     return (token_grad, gate_grad, grad_gate[None], grad_up[None], grad_down[None], router_grad)
 
 
+def gather_rows(part):
+    rows = lax.all_gather(part, "ep", axis=0, tiled=True)
+    return lax.all_gather(rows, "tp", axis=1, tiled=True)
+
+
+def scatter_rows(partial):
+    by_col = lax.psum_scatter(partial, "tp", scatter_dimension=1, tiled=True)
+    return lax.psum_scatter(by_col, "ep", scatter_dimension=0, tiled=True)
+
+
+def dense_shards(tokens, cotangent, routes, router, w_gate, w_up, w_down):
+    highest = lax.Precision.HIGHEST
+    ep_count = lax.axis_size("ep")
+    tp_count = lax.axis_size("tp")
+    experts = ep_count // BLOCKS
+    tok_rows, width = tokens.shape
+    col_width = width // tp_count
+    ep_index = lax.axis_index("ep")
+    tp_index = lax.axis_index("tp")
+    expert = ep_index // BLOCKS
+    w_gate, w_up, w_down = w_gate[0], w_up[0], w_down[0]
+
+    routes_t = lax.all_gather(routes.T.astype(jnp.float32), "ep", axis=1, tiled=True)
+    routes_t = routes_t.astype(jnp.int32)
+    tok_part = lax.dynamic_slice_in_dim(tokens, tp_index * col_width, col_width, 1)
+    cot_part = lax.dynamic_slice_in_dim(cotangent, tp_index * col_width, col_width, 1)
+    tok_all = gather_rows(tok_part)
+    cot_all = gather_rows(cot_part)
+
+    logits = lax.dot_general(
+        router, tok_all, (((0,), (1,)), ((), ())), preferred_element_type=jnp.float32
+    )
+    labels = jnp.arange(experts, dtype=jnp.int32)[:, None]
+    picked = [(routes_t[k][None, :] == labels).astype(jnp.float32) for k in range(2)]
+    chosen = [jnp.sum(p * logits, axis=0) for p in picked]
+    margin = chosen[0] - chosen[1]
+    weights = [jax.nn.sigmoid(margin), jax.nn.sigmoid(-margin)]
+    sent = [w.astype(jnp.bfloat16).astype(jnp.float32) for w in weights]
+    mine = [(routes_t[k] == expert).astype(jnp.float32) for k in range(2)]
+    gate_col = (mine[0] * sent[0] + mine[1] * sent[1])[:, None]
+
+    pre_gate = jnp.dot(tok_all, w_gate, preferred_element_type=jnp.float32)
+    pre_up = jnp.dot(tok_all, w_up, preferred_element_type=jnp.float32)
+    back_grad = lax.dot_general(
+        cot_all, w_down, (((1,), (1,)), ((), ())), preferred_element_type=jnp.float32
+    )
+    sig_gate = jax.nn.sigmoid(pre_gate)
+    active = pre_gate * sig_gate
+    hidden = (active * pre_up).astype(jnp.bfloat16)
+    gate_terms = jnp.sum(hidden.astype(jnp.float32) * back_grad, axis=1)
+    scaled_back = gate_col * back_grad
+    d_gate = (scaled_back * pre_up * sig_gate * (1.0 + pre_gate * (1.0 - sig_gate))).astype(
+        jnp.bfloat16
+    )
+    d_up = (scaled_back * active).astype(jnp.bfloat16)
+    scaled_cot = (gate_col * cot_all.astype(jnp.float32)).astype(jnp.bfloat16)
+
+    contract_hidden = (((1,), (1,)), ((), ()))
+    partial_dx = lax.dot_general(
+        d_gate, w_gate, contract_hidden, preferred_element_type=jnp.float32
+    )
+    partial_dx = partial_dx + lax.dot_general(
+        d_up, w_up, contract_hidden, preferred_element_type=jnp.float32
+    )
+    routed_dx = scatter_rows(partial_dx.astype(jnp.bfloat16))
+    gate_sum = lax.psum(
+        jnp.stack([mine[0] * gate_terms, mine[1] * gate_terms]), ("ep", "tp")
+    )
+
+    contract_rows = (((0,), (0,)), ((), ()))
+    grad_gate = lax.dot_general(
+        tok_all, d_gate, contract_rows, preferred_element_type=jnp.float32
+    ).astype(jnp.bfloat16)
+    grad_up = lax.dot_general(
+        tok_all, d_up, contract_rows, preferred_element_type=jnp.float32
+    ).astype(jnp.bfloat16)
+    grad_down = lax.dot_general(
+        hidden, scaled_cot, contract_rows, preferred_element_type=jnp.float32
+    ).astype(jnp.bfloat16)
+
+    lead = weights[0] * weights[1] * (gate_sum[0] - gate_sum[1])
+    logit_grad = (picked[0] - picked[1]) * lead[None, :]
+    own_logit = lax.dynamic_slice_in_dim(logit_grad, ep_index * tok_rows, tok_rows, 1)
+    gate_grad = lax.dynamic_slice_in_dim(gate_sum, ep_index * tok_rows, tok_rows, 1).T
+    router_cols = lax.dynamic_slice_in_dim(router, tp_index * col_width, col_width, 0)
+    token_grad = (
+        routed_dx.astype(jnp.float32)
+        + lax.dot_general(
+            own_logit,
+            router_cols.astype(jnp.float32),
+            (((0,), (1,)), ((), ())),
+            precision=highest,
+        )
+    ).astype(jnp.bfloat16)
+    seg = width // (ep_count * tp_count)
+    own_cols = lax.dynamic_slice_in_dim(
+        tok_all, (ep_index * tp_count + tp_index) * seg, seg, 1
+    ).astype(jnp.float32)
+    router_grad = lax.dot_general(
+        logit_grad, own_cols, (((1,), (0,)), ((), ())), precision=highest
+    ).T
+    return (token_grad, gate_grad, grad_gate[None], grad_up[None], grad_down[None], router_grad)
+
+
+def shards(tokens, cotangent, routes, router, w_gate, w_up, w_down):
+    slots = 3 * routes.shape[1] * BLOCKS
+    dense = slots >= lax.axis_size("ep")
+    path = dense_shards if dense else routed_shards
+    return path(tokens, cotangent, routes, router, w_gate, w_up, w_down)
+
+
 def solution(mesh):
     placed = (
         P("ep", None),

time: 326 us -> 303 us (0.929)
  starting transfers between devices: 11.3 us -> 0.24 us
  blocking collectives: 65.4 us -> 58.3 us
  other arithmetic: 5.65 us -> 0.07 us
  matrix products: 39.1 us -> 43.9 us
    unnamed x5 -> x6, waiting for transfers between devices: 122 us -> 0.1 us
    all_gather x2 -> x4, waiting for transfers between devices: 23.9 us -> 126 us  [the longest x2 84.7 us: gather_rows(): rows = lax.all_gather(part, 'ep', axis=0, tiled=True)]
    all_to_all x3 -> x0, blocking collectives: 59.5 us -> none  [the longest x1 27.3 us: shards(): lax.all_to_all(pack_rows(tok_part), 'ep', split_axis=0, concat_axis=0, ti...]
    psum x1, blocking collectives: 5.86 us -> 39.9 us  [dense_shards(): lax.psum(jnp.stack([mine[0] * gate_terms, mine[1] * gate_terms]), ('ep',...]
    reduce_scatter x1 -> x2, waiting for transfers between devices: 33.2 us -> 56.4 us  [the longest x1 53 us: scatter_rows(): return lax.psum_scatter(by_col, 'ep', scatter_dimension=0, tiled=True)]
    all_gather x0 -> x1, blocking collectives: none -> 18.3 us  [dense_shards(): lax.all_gather(routes.T.astype(jnp.float32), 'ep', axis=1, tiled=True)]
    all_to_all x2 -> x0, starting transfers between devices: 11.2 us -> none  [the longest x1 5.66 us: shards(): lax.all_to_all(gate_sums.astype(jnp.bfloat16), 'ep', split_axis=0, concat...]
    dot_general x15 -> x11, matrix products: 37.3 us -> 43.9 us  [the longest x1 8.32 us: dense_shards(): lax.dot_general(cot_all, w_down, (((1,), (1,)), ((), ())), preferred_elem...]
  transfers between devices with their start and end apart: 6 -> 6, of which waited for: 5 -> 6; matrix products, arithmetic and copies ran while one was open for 8% -> 10% of each run, Pallas kernels for 0% -> 0%
where the time goes in v1:
time: 303 us
  waiting for transfers between devices  182 us (60%)
  blocking collectives  58.3 us (19%)
  matrix products  43.9 us (14%)
  between operations  14.3 us (5%)
  local copies, waits for them, and re-layouts  3.91 us (1%)
    all_gather x2, waiting for transfers between devices, gather_rows(): rows = lax.all_gather(part, 'ep', axis=0, tiled=True)  84.7 us
    reduce_scatter x1, waiting for transfers between devices, scatter_rows(): return lax.psum_scatter(by_col, 'ep', scatter_dimension=0, tiled=True)  53 us
    all_gather x2, waiting for transfers between devices, gather_rows(): return lax.all_gather(rows, 'tp', axis=1, tiled=True)  41.1 us
    psum x1, blocking collectives, dense_shards(): lax.psum(jnp.stack([mine[0] * gate_terms, mine[1] * gate_terms]), ('ep',...  39.9 us
    all_gather x1, blocking collectives, dense_shards(): lax.all_gather(routes.T.astype(jnp.float32), 'ep', axis=1, tiled=True)  18.3 us
    dot_general x1, matrix products, dense_shards(): lax.dot_general(cot_all, w_down, (((1,), (1,)), ((), ())), preferred_elem...  8.32 us
    dot_general x1, matrix products, dense_shards(): lax.dot_general(tok_all, d_gate, contract_rows, preferred_element_type=jn...  6.36 us
  transfers between devices with their start and end apart: 6, of which 6 were waited for; matrix products, arithmetic and copies ran while one was open for 10% of the time, Pallas kernels for 0%

profile of v1, /device:TPU:0, one launch (start us, length us, event | category | flops | bytes accessed | tf_op | source)
XLA Modules:
  0.0 303.0 jit_solution(7012524095717071216)
XLA Ops:
  7.3 1.7 constant_dynamic-slice_fusion.2
  9.0 0.0 all-gather.9.cloned.1.call-start
  9.0 1.6 constant_dynamic-slice_fusion.1
  10.7 43.1 %all-gather.5.cloned.1.call-done = bf16[1024,512]{1,0:T(8,128)(2,1)} async-done(((bf16[128,512]{1,0:T(8,128)(2,1)}), bf16[1024,512]{1,0:T(8,128)(2,1)}) %all-gather.5.cloned.1.call-update) | async-done | bytes 1048592 | tf_op jit(solution)/shard_map/all_gather | solution.py:163
  53.8 41.6 %all-gather.9.cloned.1.call-done = bf16[1024,512]{1,0:T(8,128)(2,1)} async-done(((bf16[128,512]{1,0:T(8,128)(2,1)}), bf16[1024,512]{1,0:T(8,128)(2,1)}) %all-gather.9.cloned.1.call-update) | async-done | bytes 1048592 | tf_op jit(solution)/shard_map/all_gather | solution.py:163
  95.6 18.3 %all_gather.15 = f32[2,1024]{1,0:T(2,128)S(1)} all-gather(f32[2,128]{1,0:T(2,128)S(1)} %convert_bitcast_fusion), channel_id=1, replica_groups=mesh['ep'=8,'tp'=4] {'ep'}, dimensions={1}, use_global_device_ids=true | all-gather | bytes 9216 | tf_op jit(solution)/shard_map/all_gather | solution.py:184
  113.9 16.3 %all-gather.7.cloned.1.call-done = bf16[1024,2048]{1,0:T(8,128)(2,1)} async-done(((bf16[1024,512]{1,0:T(8,128)(2,1)}), bf16[1024,2048]{1,0:T(8,128)(2,1)}) %all-gather.7.cloned.1.call-update) | async-done | bytes 4194320 | tf_op jit(solution)/shard_map/all_gather | solution.py:164
  130.2 3.5 %select_reduce_fusion = (f32[1024]{0:T(1024)S(1)}, f32[1024]{0:T(1024)S(1)}) fusion(s32[1024]{0:T(1024)S(1)} %bitcast.48, s32[1024]{0:T(1024)S(1)} %bitcast.44, bf16[1024,2048]{1,0:T(8,128)(2,1)} %all-gather.7.cloned.1.call-done, bf16[2048,4]{0,1:T(4,128)(2,1)S(1)} %copy-done.3), kind=kOutput, calls=%fused_computation.31 | convolution fusion | flops 16799744 | bytes 4227072 | tf_op jit(solution)/shard_map/dot_general | solution.py:191
  133.8 3.8 %fusion.8 = f32[1024,512]{0,1:T(8,128)} fusion(bf16[1024,2048]{1,0:T(8,128)(2,1)S(1)} %copy-done.1, bf16[1,2048,512]{2,1,0:T(8,128)(2,1)S(1)} %copy-done), kind=kOutput, calls=%fused_computation.12 | convolution fusion | flops 2147483648 | bytes 8388608 | tf_op jit(solution)/shard_map/dot_general | solution.py:203
  137.6 3.8 %fusion.11 = f32[1024,512]{0,1:T(8,128)} fusion(bf16[1024,2048]{1,0:T(8,128)(2,1)S(1)} %copy-done.1, bf16[1,2048,512]{2,1,0:T(8,128)(2,1)S(1)} %copy-done.6), kind=kOutput, calls=%fused_computation.15 | convolution fusion | flops 2147483648 | bytes 8388608 | tf_op jit(solution)/shard_map/dot_general | solution.py:204
  141.4 24.8 %all-gather.11.cloned.1.call-done = bf16[1024,2048]{1,0:T(8,128)(2,1)} async-done(((bf16[1024,512]{1,0:T(8,128)(2,1)}), bf16[1024,2048]{1,0:T(8,128)(2,1)}) %all-gather.11.cloned.1.call-update) | async-done | bytes 4194320 | tf_op jit(solution)/shard_map/all_gather | solution.py:164
  166.1 8.3 %multiply_reduce_fusion = (f32[1024]{0:T(1024)S(1)}, bf16[1024,512]{0,1:T(8,128)(2,1)}, bf16[1024,512]{0,1:T(8,128)(2,1)S(1)}, bf16[1024,512]{0,1:T(8,128)(2,1)S(1)}) fusion(f32[1024,512]{0,1:T(8,128)} %fusion.11, f32[1024,512]{0,1:T(8,128)} %fusion.8, f32[1024]{0:T(1024)S(1)} %get-tuple-element.15, bf16[1024,2048]{1,0:T(8,128)(2,1)} %all-gather.11.cloned.1.call-done, ...), kind=kOutput, calls=%fused_computation.19 | convolution fusion | flops 2157444096 | bytes 13639680 | tf_op jit(solution)/shard_map/dot_general | solution.py:205
  174.5 2.4 fusion.6
  176.9 4.6 %add_convert_fusion = bf16[1024,2048]{1,0:T(8,128)(2,1)} fusion(f32[1024,2048]{1,0:T(8,128)S(1)} %fusion.6, bf16[1024,512]{0,1:T(8,128)(2,1)S(1)} %get-tuple-element.11, bf16[1,2048,512]{2,1,0:T(8,128)(2,1)S(1)} %copy-done.7), kind=kOutput, calls=%fused_computation.1 | convolution fusion | flops 2151677952 | bytes 15728640 | tf_op jit(solution)/shard_map/dot_general | solution.py:223
  181.5 0.0 reduce-scatter.5.cloned.1.call-start
  181.6 39.9 %psum.7 = f32[2,1024]{1,0:T(2,128)S(1)} all-reduce(f32[2,1024]{1,0:T(2,128)S(1)} %pad_maximum_fusion), channel_id=1, replica_groups=mesh['ep'=8,'tp'=4] {'ep','tp'}, use_global_device_ids=true, to_apply=%region_5.6 | all-reduce | flops 2048 | bytes 16384 | tf_op jit(solution)/shard_map/psum | solution.py:227
  221.5 1.9 fusion.17
  223.4 3.4 %reduce-scatter.3.cloned.1.call-done = bf16[1024,512]{1,0:T(8,128)(2,1)} async-done(((bf16[1024,2048]{1,0:T(8,128)(2,1)}), bf16[1024,512]{1,0:T(8,128)(2,1)}) %reduce-scatter.3.cloned.1.call-update) | async-done | bytes 1048592 | tf_op jit(solution)/shard_map/reduce_scatter | solution.py:168
  226.8 0.6 fusion.24
  227.4 6.4 %fusion.4 = bf16[1,2048,512]{2,1,0:T(8,128)(2,1)} fusion(bf16[1024,2048]{1,0:T(8,128)(2,1)} %all-gather.7.cloned.1.call-done, bf16[1024,512]{0,1:T(8,128)(2,1)} %copy-done.8), kind=kOutput, calls=%fused_computation.8 | convolution fusion | flops 2148532224 | bytes 7340032 | tf_op jit(solution)/shard_map/dot_general | solution.py:232
  233.8 3.7 %fusion.5 = bf16[1,2048,512]{2,1,0:T(8,128)(2,1)} fusion(bf16[1024,2048]{1,0:T(8,128)(2,1)S(1)} %copy-done.2, bf16[1024,512]{0,1:T(8,128)(2,1)S(1)} %get-tuple-element.11), kind=kOutput, calls=%fused_computation.9 | convolution fusion | flops 2148532224 | bytes 7340032 | tf_op jit(solution)/shard_map/dot_general | solution.py:235
  237.5 3.8 %fusion.3 = bf16[1,512,2048]{2,1,0:T(8,128)(2,1)} fusion(bf16[1024,512]{0,1:T(8,128)(2,1)S(1)} %copy-done.9, bf16[1024,2048]{1,0:T(8,128)(2,1)S(1)} %copy-done.5, f32[1024]{0:T(1024)S(1)} %get-tuple-element.15), kind=kOutput, calls=%fused_computation.7 | convolution fusion | flops 2154823680 | bytes 7344128 | tf_op jit(solution)/shard_map/dot_general | solution.py:238
  241.2 53.0 %reduce-scatter.5.cloned.1.call-done = bf16[128,512]{1,0:T(8,128)(2,1)} async-done(((bf16[1024,512]{1,0:T(8,128)(2,1)}), bf16[128,512]{1,0:T(8,128)(2,1)}) %reduce-scatter.5.cloned.1.call-update) | async-done | bytes 131088 | tf_op jit(solution)/shard_map/reduce_scatter | solution.py:169
  294.2 1.9 fusion.16
  (38 shorter events, 0.4 us)
Async XLA Ops:
  7.2 126.6 %copy-start = (bf16[1,2048,512]{2,1,0:T(8,128)(2,1)S(1)}, bf16[1,2048,512]{2,1,0:T(8,128)(2,1)}, u32[]{:S(2)}) copy-start(bf16[1,2048,512]{2,1,0:T(8,128)(2,1)} %param.11) | copy-start | bytes 6291460
  7.2 88.4 %copy-start.4 = (s32[128,2]{0,1:T(2,128)S(1)}, s32[128,2]{0,1:T(2,128)}, u32[]{:S(2)}) copy-start(s32[128,2]{0,1:T(2,128)} %param.9) | copy-start | bytes 3076
  7.2 123.0 %copy-start.3 = (bf16[2048,4]{0,1:T(4,128)(2,1)S(1)}, bf16[2048,4]{0,1:T(4,128)(2,1)}, u32[]{:S(2)}) copy-start(bf16[2048,4]{0,1:T(4,128)(2,1)} %param.10) | copy-start | bytes 49156
  7.2 46.5 %all-gather.5.cloned.1.call-start = ((), (), s32[]{:S(2)}) async-start(), calls=%async_computation.2 | async-start | bytes 1179648 | tf_op jit(solution)/shard_map/all_gather | solution.py:163
  9.0 86.5 %all-gather.9.cloned.1.call-start = ((), (), s32[]{:S(2)}) async-start(), calls=%async_computation.4 | async-start | bytes 1179648 | tf_op jit(solution)/shard_map/all_gather | solution.py:163
  10.6 119.6 %all-gather.7.cloned.1.call-start = ((), (), s32[]{:S(2)}) async-start(), calls=%async_computation.3 | async-start | bytes 5242880 | tf_op jit(solution)/shard_map/all_gather | solution.py:164
  53.8 112.4 %all-gather.11.cloned.1.call-start = ((), (), s32[]{:S(2)}) async-start(), calls=%async_computation.5 | async-start | bytes 5242880 | tf_op jit(solution)/shard_map/all_gather | solution.py:164
  95.5 131.3 %reduce-scatter.3.cloned.1.call-start = ((), (), s32[]{:S(2)}) async-start(), calls=%async_computation.6 | async-start | bytes 5242880 | tf_op jit(solution)/shard_map/reduce_scatter | solution.py:168
  130.2 3.6 %copy-start.1 = (bf16[1024,2048]{1,0:T(8,128)(2,1)S(1)}, bf16[1024,2048]{1,0:T(8,128)(2,1)}, u32[]{:S(2)}) copy-start(bf16[1024,2048]{1,0:T(8,128)(2,1)} %all-gather.7.cloned.1.call-done) | copy-start | bytes 12582916
  133.8 3.8 %copy-start.6 = (bf16[1,2048,512]{2,1,0:T(8,128)(2,1)S(1)}, bf16[1,2048,512]{2,1,0:T(8,128)(2,1)}, u32[]{:S(2)}) copy-start(bf16[1,2048,512]{2,1,0:T(8,128)(2,1)} %param.12) | copy-start | bytes 6291460
  174.5 2.4 copy-start.8
  174.5 2.4 copy-start.7
  181.5 112.8 %reduce-scatter.5.cloned.1.call-start = ((), (), s32[]{:S(2)}) async-start(), calls=%async_computation.7 | async-start | bytes 1179648 | tf_op jit(solution)/shard_map/reduce_scatter | solution.py:169
  227.4 6.4 %copy-start.2 = (bf16[1024,2048]{1,0:T(8,128)(2,1)S(1)}, bf16[1024,2048]{1,0:T(8,128)(2,1)}, u32[]{:S(2)}) copy-start(bf16[1024,2048]{1,0:T(8,128)(2,1)} %all-gather.7.cloned.1.call-done) | copy-start | bytes 12582916
  233.7 3.7 %copy-start.5 = (bf16[1024,2048]{1,0:T(8,128)(2,1)S(1)}, bf16[1024,2048]{1,0:T(8,128)(2,1)}, u32[]{:S(2)}) copy-start(bf16[1024,2048]{1,0:T(8,128)(2,1)} %all-gather.11.cloned.1.call-done) | copy-start | bytes 12582916
  233.7 3.7 %copy-start.9 = (bf16[1024,512]{0,1:T(8,128)(2,1)S(1)}, bf16[1024,512]{0,1:T(8,128)(2,1)}, u32[]{:S(2)}) copy-start(bf16[1024,512]{0,1:T(8,128)(2,1)} %get-tuple-element.9) | copy-start | bytes 3145732
Sparse Core Ops, SparseCore 0:
  10.7 42.9 all-gather.4
  56.4 38.9 all-gather.8
  97.0 33.1 all-gather.6
  131.6 34.4 all-gather.10
  181.6 45.1 reduce-scatter.2
  230.0 64.1 reduce-scatter.4

commit v2 on v1

--- a/solution.py
+++ b/solution.py
@@ -1,9 +1,13 @@
 import jax
 import jax.numpy as jnp
 from jax import lax
+from jax.experimental import pallas as pl
+from jax.experimental.pallas import tpu as pltpu
 from jax.sharding import PartitionSpec as P
 
 BLOCKS = 2
+CORES = 2
+MESH = pl.DeviceIdType.MESH
 
 
 def build_slots(block_routes, experts, capacity):
@@ -159,14 +163,237 @@
     return (token_grad, gate_grad, grad_gate[None], grad_up[None], grad_down[None], router_grad)
 
 
-def gather_rows(part):
-    rows = lax.all_gather(part, "ep", axis=0, tiled=True)
-    return lax.all_gather(rows, "tp", axis=1, tiled=True)
+class Place:
+    def __init__(self):
+        self.line = lax.axis_size("ep") // BLOCKS
+        ep, self.tp = lax.axis_index("ep"), lax.axis_index("tp")
+        self.z, self.x = ep // BLOCKS, ep % BLOCKS
+        self.y, self.c = self.tp // CORES, self.tp % CORES
+
+    def ep(self, z, x):
+        return z * BLOCKS + x
+
+    def on_line(self, step):
+        z = (self.z + step) % self.line
+        return {"ep": self.ep(z, self.x), "tp": self.tp}
+
+    def across(self):
+        return {"ep": self.ep(self.z, 1 - self.x), "tp": self.tp}
+
+    def other_plane(self):
+        return {"ep": self.ep(self.z, self.x), "tp": (1 - self.y) * CORES + self.c}
+
+    def other_core(self):
+        return {"ep": self.ep(self.z, self.x), "tp": self.y * CORES + 1 - self.c}
+
+    def greet(self):
+        barrier = pltpu.get_barrier_semaphore()
+        peers = [self.on_line(step) for step in range(1, self.line)]
+        peers += [self.across(), self.other_plane(), self.other_core()]
+        for peer in peers:
+            pl.semaphore_signal(barrier, inc=1, device_id=peer, device_id_type=MESH)
+        pl.semaphore_wait(barrier, len(peers))
+
+
+def remote(src, dst, sems, index, peer):
+    return pltpu.make_async_remote_copy(
+        src_ref=src,
+        dst_ref=dst,
+        send_sem=sems.at[(0,) + index],
+        recv_sem=sems.at[(1,) + index],
+        device_id=peer,
+        device_id_type=MESH,
+    )
+
+
+def gather_kernel(
+    tok_ref, cot_ref, tok_out, cot_out, z_sems, x_sems, y_sems, c_sems, own_sems
+):
+    at = Place()
+    line = at.line
+    width = tok_ref.shape[1]
+    half = width // CORES
+    unit = half // 4
+    ins, outs = (tok_ref, cot_ref), (tok_out, cot_out)
+    own = at.ep(at.z, at.x)
+    window = pl.ds(pl.multiple_of(at.c * half + at.y * unit, unit), half - unit)
+    outer = pl.ds(pl.multiple_of(at.c * half + at.y * (half - unit), unit), unit)
+    mine = pl.ds(pl.multiple_of(at.c * half, half), half)
+    at.greet()
+
+    started = []
+
+    def send(src, dst, sems, index, peer):
+        copy = remote(src, dst, sems, index, peer)
+        copy.start()
+        started.append(copy)
+
+    for step in range(1, line):
+        for i in range(2):
+            send(
+                ins[i].at[:, window], outs[i].at[own, :, window],
+                z_sems, (step - 1, i), at.on_line(step),
+            )
+    for i in range(2):
+        send(ins[i].at[:, window], outs[i].at[own, :, window], x_sems, (0, i), at.across())
+    keep = [pltpu.make_async_copy(ins[i], outs[i].at[own], own_sems.at[i]) for i in range(2)]
+    for copy in keep:
+        copy.start()
+
+    def arrived(sems, index, i, block, columns):
+        ref = outs[i].at[block, :, columns]
+        remote(ref, ref, sems, index, at.across()).wait_recv()
+
+    def pass_on(block, columns, sems, index, peer, i):
+        ref = outs[i].at[block, :, columns]
+        send(ref, ref, sems, index, peer)
+
+    blocks = []
+    for step in range(1, line):
+        block = at.ep((at.z - step + line) % line, at.x)
+        blocks.append(block)
+        for i in range(2):
+            arrived(z_sems, (step - 1, i), i, block, window)
+            pass_on(block, window, x_sems, (step, i), at.across(), i)
+            pass_on(block, outer, y_sems, (step - 1, i), at.other_plane(), i)
+    for step in range(line):
+        block = at.ep((at.z - step + line) % line, 1 - at.x)
+        blocks.append(block)
+        for i in range(2):
+            arrived(x_sems, (step, i), i, block, window)
+            pass_on(block, outer, y_sems, (line - 1 + step, i), at.other_plane(), i)
+    inner = pl.ds(pl.multiple_of(at.c * half + (1 - at.y) * (half - unit), unit), unit)
+    for k, block in enumerate(blocks):
+        for i in range(2):
+            arrived(y_sems, (k, i), i, block, inner)
+            pass_on(block, mine, c_sems, (k, i), at.other_core(), i)
+    theirs = pl.ds(pl.multiple_of((1 - at.c) * half, half), half)
+    for k, block in enumerate(blocks):
+        for i in range(2):
+            arrived(c_sems, (k, i), i, block, theirs)
+    for copy in keep:
+        copy.wait()
+    for copy in started:
+        copy.wait_send()
+
+
+def gather_rows(tokens, cotangent):
+    ep_count = lax.axis_size("ep")
+    line = ep_count // BLOCKS
+    rows, width = tokens.shape
+    whole = jax.ShapeDtypeStruct((ep_count, rows, width), tokens.dtype)
+    dma = pltpu.SemaphoreType.DMA
+    tok_all, cot_all = pl.pallas_call(
+        gather_kernel,
+        out_shape=(whole, whole),
+        in_specs=[pl.BlockSpec(memory_space=pltpu.VMEM)] * 2,
+        out_specs=[pl.BlockSpec(memory_space=pltpu.VMEM)] * 2,
+        scratch_shapes=[
+            dma((2, line - 1, 2)),
+            dma((2, line, 2)),
+            dma((2, ep_count - 1, 2)),
+            dma((2, ep_count - 1, 2)),
+            dma((2,)),
+        ],
+        compiler_params=pltpu.CompilerParams(collective_id=0, has_side_effects=True),
+    )(tokens, cotangent)
+    return tok_all.reshape(-1, width), cot_all.reshape(-1, width)
+
+
+def scatter_kernel(
+    dx_ref, out_ref, c_recv, y_send, y_recv, x_send, x_recv, z_send, z_recv, total,
+    c_sems, y_sems, x_sems, z_sems,
+):
+    at = Place()
+    line = at.line
+    part = out_ref.shape[1]
+
+    def columns(plane, core):
+        return pl.ds(pl.multiple_of((plane * CORES + core) * part, part), part)
+
+    def f32(value):
+        return value.astype(jnp.float32)
+
+    at.greet()
+    started = []
+
+    def send(src, dst, sems, index, peer):
+        copy = remote(src, dst, sems, index, peer)
+        copy.start()
+        started.append(copy)
+
+    def arrived(ref, sems, index):
+        remote(ref, ref, sems, index, at.across()).wait_recv()
+
+    blocks = [
+        at.ep((at.z + 1 + j) % line, x) for x in (1 - at.x, at.x) for j in range(line)
+    ]
+    for k, block in enumerate(blocks):
+        for p in range(2):
+            send(
+                dx_ref.at[block, :, columns(p, 1 - at.c)], c_recv.at[k, p],
+                c_sems, (k, p), at.other_core(),
+            )
+    for k, block in enumerate(blocks):
+        for p in range(2):
+            arrived(c_recv.at[k, p], c_sems, (k, p))
+        y_send[k] = (
+            f32(dx_ref[block, :, columns(1 - at.y, at.c)]) + f32(c_recv[k, 1 - at.y])
+        ).astype(y_send.dtype)
+        send(y_send.at[k], y_recv.at[k], y_sems, (k,), at.other_plane())
+        total[k] = f32(dx_ref[block, :, columns(at.y, at.c)]) + f32(c_recv[k, at.y])
+    for j in range(line):
+        arrived(y_recv.at[j], y_sems, (j,))
+        x_send[j] = (total[j] + f32(y_recv[j])).astype(x_send.dtype)
+        send(x_send.at[j], x_recv.at[j], x_sems, (j,), at.across())
+    for j in range(line):
+        k = line + j
+        arrived(y_recv.at[k], y_sems, (k,))
+        arrived(x_recv.at[j], x_sems, (j,))
+        summed = total[k] + f32(y_recv[k]) + f32(x_recv[j])
+        if j < line - 1:
+            z_send[j] = summed.astype(z_send.dtype)
+            send(z_send.at[j], z_recv.at[j], z_sems, (j,), at.on_line(1 + j))
+        else:
+            out_ref[...] = summed
+    for j in range(line - 1):
+        arrived(z_recv.at[j], z_sems, (j,))
+        out_ref[...] += f32(z_recv[j])
+    for copy in started:
+        copy.wait_send()
 
 
 def scatter_rows(partial):
-    by_col = lax.psum_scatter(partial, "tp", scatter_dimension=1, tiled=True)
-    return lax.psum_scatter(by_col, "ep", scatter_dimension=0, tiled=True)
+    ep_count, tp_count = lax.axis_size("ep"), lax.axis_size("tp")
+    line = ep_count // BLOCKS
+    width = partial.shape[1]
+    rows, part = partial.shape[0] // ep_count, width // tp_count
+    dma = pltpu.SemaphoreType.DMA
+
+    def slots(*lead, kind=partial.dtype):
+        return pltpu.VMEM(lead + (rows, part), kind)
+
+    return pl.pallas_call(
+        scatter_kernel,
+        out_shape=jax.ShapeDtypeStruct((rows, part), jnp.float32),
+        in_specs=[pl.BlockSpec(memory_space=pltpu.VMEM)],
+        out_specs=pl.BlockSpec(memory_space=pltpu.VMEM),
+        scratch_shapes=[
+            slots(ep_count, 2),
+            slots(ep_count),
+            slots(ep_count),
+            slots(line),
+            slots(line),
+            slots(line - 1),
+            slots(line - 1),
+            slots(ep_count, kind=jnp.float32),
+            dma((2, ep_count, 2)),
+            dma((2, ep_count)),
+            dma((2, line)),
+            dma((2, line - 1)),
+        ],
+        compiler_params=pltpu.CompilerParams(collective_id=1, has_side_effects=True),
+    )(partial.reshape(ep_count, rows, width))
 
 
 def dense_shards(tokens, cotangent, routes, router, w_gate, w_up, w_down):
@@ -183,10 +410,7 @@
 
     routes_t = lax.all_gather(routes.T.astype(jnp.float32), "ep", axis=1, tiled=True)
     routes_t = routes_t.astype(jnp.int32)
-    tok_part = lax.dynamic_slice_in_dim(tokens, tp_index * col_width, col_width, 1)
-    cot_part = lax.dynamic_slice_in_dim(cotangent, tp_index * col_width, col_width, 1)
-    tok_all = gather_rows(tok_part)
-    cot_all = gather_rows(cot_part)
+    tok_all, cot_all = gather_rows(tokens, cotangent)
 
     logits = lax.dot_general(
         router, tok_all, (((0,), (1,)), ((), ())), preferred_element_type=jnp.float32
@@ -245,7 +469,7 @@
     gate_grad = lax.dynamic_slice_in_dim(gate_sum, ep_index * tok_rows, tok_rows, 1).T
     router_cols = lax.dynamic_slice_in_dim(router, tp_index * col_width, col_width, 0)
     token_grad = (
-        routed_dx.astype(jnp.float32)
+        routed_dx
         + lax.dot_general(
             own_logit,
             router_cols.astype(jnp.float32),
@@ -265,7 +489,7 @@
 
 def shards(tokens, cotangent, routes, router, w_gate, w_up, w_down):
     slots = 3 * routes.shape[1] * BLOCKS
-    dense = slots >= lax.axis_size("ep")
+    dense = slots >= lax.axis_size("ep") and lax.axis_size("tp") == 2 * CORES
     path = dense_shards if dense else routed_shards
     return path(tokens, cotangent, routes, router, w_gate, w_up, w_down)
 

time: 303 us -> 196 us (0.65)
  waiting for transfers between devices: 182 us -> 0 us
  Pallas kernels: 0 us -> 84.8 us
  between operations: 14.3 us -> 0.83 us
  blocking collectives: 58.3 us -> 70.4 us
  matrix products: 43.9 us -> 37 us
    all_gather x4 -> x0, waiting for transfers between devices: 126 us -> none  [the longest x2 84.7 us: gather_rows(): rows = lax.all_gather(part, 'ep', axis=0, tiled=True)]
    pallas_call x0 -> x2, Pallas kernels: none -> 84.8 us  [the longest x1 48.4 us: gather_rows(): pl.pallas_call(gather_kernel, out_shape=(whole, whole), in_specs=[pl.Bloc...]
    reduce_scatter x2 -> x0, waiting for transfers between devices: 56.4 us -> none  [the longest x1 53 us: scatter_rows(): return lax.psum_scatter(by_col, 'ep', scatter_dimension=0, tiled=True)]
    psum x1, blocking collectives: 39.9 us -> 48 us  [dense_shards(): lax.psum(jnp.stack([mine[0] * gate_terms, mine[1] * gate_terms]), ('ep',...]
    dot_general x1, matrix products: 8.32 us -> 4.21 us  [dense_shards(): lax.dot_general(cot_all, w_down, (((1,), (1,)), ((), ())), preferred_elem...]
    all_gather x1, blocking collectives: 18.3 us -> 22.4 us  [dense_shards(): lax.all_gather(routes.T.astype(jnp.float32), 'ep', axis=1, tiled=True)]
    dynamic_slice x2 -> x0, local copies, waits for them, and re-layouts: 3.28 us -> none  [the longest x1 1.71 us: dense_shards(): lax.dynamic_slice_in_dim(tokens, tp_index * col_width, col_width, 1)]
  transfers between devices with their start and end apart: 6 -> 0, of which waited for: 6 -> 0; matrix products, arithmetic and copies ran while one was open for 10% -> 0% of each run, Pallas kernels for 0% -> 0%
where the time goes in v2:
time: 196 us; the launch traced here: 195 us
  Pallas kernels  84.8 us (43%)
  blocking collectives  70.4 us (36%)
  matrix products  37 us (19%)
    pallas_call x1, Pallas kernels, gather_rows(): pl.pallas_call(gather_kernel, out_shape=(whole, whole), in_specs=[pl.Bloc...  48.4 us
    psum x1, blocking collectives, dense_shards(): lax.psum(jnp.stack([mine[0] * gate_terms, mine[1] * gate_terms]), ('ep',...  48 us
    pallas_call x1, Pallas kernels, scatter_rows(): pl.pallas_call(scatter_kernel, out_shape=jax.ShapeDtypeStruct((rows, part...  36.4 us
    all_gather x1, blocking collectives, dense_shards(): lax.all_gather(routes.T.astype(jnp.float32), 'ep', axis=1, tiled=True)  22.4 us
    dot_general x1, matrix products, dense_shards(): lax.dot_general(tok_all, d_gate, contract_rows, preferred_element_type=jn...  6.36 us
    dot_general x1, matrix products, dense_shards(): lax.dot_general(d_up, w_up, contract_hidden, preferred_element_type=jnp.f...  4.33 us
    dot_general x1, matrix products, dense_shards(): lax.dot_general(cot_all, w_down, (((1,), (1,)), ((), ())), preferred_elem...  4.21 us

profile of v2, /device:TPU:0, one launch (start us, length us, event | category | flops | bytes accessed | tf_op | source)
XLA Modules:
  0.0 195.0 jit_solution(7457966767711008185)
XLA Ops:
  0.6 0.0 copy-start
  0.7 0.8 convert_bitcast_fusion
  1.5 22.4 %all_gather.3 = f32[2,1024]{1,0:T(2,128)S(1)} all-gather(f32[2,128]{1,0:T(2,128)S(1)} %convert_bitcast_fusion), channel_id=1, replica_groups=mesh['ep'=8,'tp'=4] {'ep'}, dimensions={1}, use_global_device_ids=true | all-gather | bytes 9216 | tf_op jit(solution)/shard_map/all_gather | solution.py:411
  23.9 48.4 %shard_map.118 = (bf16[8,128,2048]{2,1,0:T(8,128)(2,1)}, bf16[8,128,2048]{2,1,0:T(8,128)(2,1)}) custom-call(bf16[128,2048]{1,0:T(8,128)(2,1)} %tok_ref.1, bf16[128,2048]{1,0:T(8,128)(2,1)} %cot_ref.1), custom_call_target="tpu_custom_call" | custom-call | tf_op jit(solution)/shard_map/pallas_call | solution.py:286
  72.3 3.5 %select_reduce_fusion = (f32[1024]{0:T(1024)S(1)}, f32[1024]{0:T(1024)S(1)}) fusion(s32[1024]{0:T(1024)S(1)} %bitcast.58, s32[1024]{0:T(1024)S(1)} %bitcast.54, bf16[1024,2048]{1,0:T(8,128)(2,1)} %bitcast.47, bf16[2048,4]{0,1:T(4,128)(2,1)} %param.10), kind=kOutput, calls=%fused_computation.31 | convolution fusion | flops 16799744 | bytes 4227072 | tf_op jit(solution)/shard_map/dot_general | solution.py:415
  75.9 0.0 copy-done
  75.9 0.0 copy-done.1
  75.9 0.0 copy-start.5
  75.9 2.4 %fusion.8 = f32[1024,512]{0,1:T(8,128)S(1)} fusion(bf16[1024,2048]{1,0:T(8,128)(2,1)S(1)} %bitcast.50, bf16[1,2048,512]{2,1,0:T(8,128)(2,1)S(1)} %copy-done), kind=kOutput, calls=%fused_computation.12 | convolution fusion | flops 2147483648 | bytes 8388608 | tf_op jit(solution)/shard_map/dot_general | solution.py:427
  78.3 0.0 copy-done.5
  78.3 0.0 copy-start.4
  78.3 2.4 %fusion.11 = f32[1024,512]{0,1:T(8,128)S(1)} fusion(bf16[1024,2048]{1,0:T(8,128)(2,1)S(1)} %bitcast.51, bf16[1,2048,512]{2,1,0:T(8,128)(2,1)S(1)} %copy-done.5), kind=kOutput, calls=%fused_computation.15 | convolution fusion | flops 2147483648 | bytes 8388608 | tf_op jit(solution)/shard_map/dot_general | solution.py:428
  80.7 0.5 copy-done.4
  81.2 4.2 %multiply_reduce_fusion = (f32[1024]{0:T(1024)S(1)}, bf16[1024,512]{0,1:T(8,128)(2,1)S(1)}, bf16[1024,512]{0,1:T(8,128)(2,1)}, bf16[1024,512]{0,1:T(8,128)(2,1)S(1)}) fusion(f32[1024,512]{0,1:T(8,128)S(1)} %fusion.11, f32[1024,512]{0,1:T(8,128)S(1)} %fusion.8, f32[1024]{0:T(1024)S(1)} %get-tuple-element.19, bf16[1024,2048]{1,0:T(8,128)(2,1)S(1)} %bitcast.66, ...), kind=kOutput, calls=%fused_computation.19 | convolution fusion | flops 2157444096 | bytes 13639680 | tf_op jit(solution)/shard_map/dot_general | solution.py:429
  85.4 3.8 %fusion.3 = bf16[1,512,2048]{2,1,0:T(8,128)(2,1)} fusion(bf16[1024,512]{0,1:T(8,128)(2,1)S(1)} %get-tuple-element.13, bf16[1024,2048]{1,0:T(8,128)(2,1)S(1)} %bitcast.67, f32[1024]{0:T(1024)S(1)} %get-tuple-element.19), kind=kOutput, calls=%fused_computation.7 | convolution fusion | flops 2154823680 | bytes 7344128 | tf_op jit(solution)/shard_map/dot_general | solution.py:462
  89.2 48.0 %psum.7 = f32[2,1024]{1,0:T(2,128)S(1)} all-reduce(f32[2,1024]{1,0:T(2,128)S(1)} %pad_maximum_fusion), channel_id=1, replica_groups=mesh['ep'=8,'tp'=4] {'ep','tp'}, use_global_device_ids=true, to_apply=%region_3.4 | all-reduce | flops 2048 | bytes 16384 | tf_op jit(solution)/shard_map/psum | solution.py:451
  137.3 0.6 dynamic-slice_bitcast_fusion
  137.8 1.9 fusion.17
  139.7 6.4 %fusion.4 = bf16[1,2048,512]{2,1,0:T(8,128)(2,1)} fusion(bf16[1024,2048]{1,0:T(8,128)(2,1)} %bitcast.49, bf16[1024,512]{0,1:T(8,128)(2,1)} %get-tuple-element.14), kind=kOutput, calls=%fused_computation.8 | convolution fusion | flops 2148532224 | bytes 7340032 | tf_op jit(solution)/shard_map/dot_general | solution.py:456
  146.1 3.8 %fusion.5 = bf16[1,2048,512]{2,1,0:T(8,128)(2,1)} fusion(bf16[1024,2048]{1,0:T(8,128)(2,1)S(1)} %bitcast.52, bf16[1024,512]{0,1:T(8,128)(2,1)S(1)} %get-tuple-element.15), kind=kOutput, calls=%fused_computation.9 | convolution fusion | flops 2148532224 | bytes 7340032 | tf_op jit(solution)/shard_map/dot_general | solution.py:459
  149.9 2.4 %fusion.6 = f32[1024,2048]{1,0:T(8,128)S(1)} fusion(bf16[1024,512]{0,1:T(8,128)(2,1)S(1)} %copy-done.7, bf16[1,2048,512]{2,1,0:T(8,128)(2,1)S(1)} %copy-done), kind=kOutput, calls=%fused_computation.10 | convolution fusion | flops 2147483648 | bytes 11534336 | tf_op jit(solution)/shard_map/dot_general | solution.py:444
  152.3 4.3 %add_convert_fusion = bf16[1024,2048]{1,0:T(8,128)(2,1)} fusion(f32[1024,2048]{1,0:T(8,128)S(1)} %fusion.6, bf16[1024,512]{0,1:T(8,128)(2,1)S(1)} %get-tuple-element.15, bf16[1,2048,512]{2,1,0:T(8,128)(2,1)S(1)} %copy-done.6), kind=kOutput, calls=%fused_computation.1 | convolution fusion | flops 2151677952 | bytes 15728640 | tf_op jit(solution)/shard_map/dot_general | solution.py:447
  156.6 36.4 %shard_map.119 = f32[128,512]{1,0:T(8,128)} custom-call(bf16[8,128,2048]{2,1,0:T(8,128)(2,1)} %bitcast.53), custom_call_target="tpu_custom_call" | custom-call | tf_op jit(solution)/shard_map/pallas_call | solution.py:376
  193.1 2.0 %fusion.16 = bf16[128,512]{1,0:T(8,128)(2,1)} fusion(f32[128,512]{1,0:T(8,128)} %shard_map.119, bf16[2048,4]{0,1:T(4,128)(2,1)} %param.10, s32[]{:T(128)S(6)} %select_n.17, f32[4,1024]{1,0:T(4,128)S(1)} %subtract_multiply_fusion, s32[]{:T(128)S(6)} %select_n.16), kind=kOutput, calls=%fused_computation.26 | convolution fusion | flops 3276800 | bytes 399368 | tf_op jit(solution)/shard_map/dot_general | solution.py:473
  (16 shorter events, 0.1 us)
Async XLA Ops:
  0.6 75.3 %copy-start = (bf16[1,2048,512]{2,1,0:T(8,128)(2,1)S(1)}, bf16[1,2048,512]{2,1,0:T(8,128)(2,1)}, u32[]{:S(2)}) copy-start(bf16[1,2048,512]{2,1,0:T(8,128)(2,1)} %param.11) | copy-start | bytes 6291460
  72.3 3.6 %copy-start.1 = (bf16[8,128,2048]{2,1,0:T(8,128)(2,1)S(1)}, bf16[8,128,2048]{2,1,0:T(8,128)(2,1)}, u32[]{:S(2)}) copy-start(bf16[8,128,2048]{2,1,0:T(8,128)(2,1)} %get-tuple-element.8) | copy-start | bytes 12582916
  75.9 2.4 %copy-start.5 = (bf16[1,2048,512]{2,1,0:T(8,128)(2,1)S(1)}, bf16[1,2048,512]{2,1,0:T(8,128)(2,1)}, u32[]{:S(2)}) copy-start(bf16[1,2048,512]{2,1,0:T(8,128)(2,1)} %param.12) | copy-start | bytes 6291460
  78.3 2.4 %copy-start.3 = (bf16[8,128,2048]{2,1,0:T(8,128)(2,1)S(1)}, bf16[8,128,2048]{2,1,0:T(8,128)(2,1)}, u32[]{:S(2)}) copy-start(bf16[8,128,2048]{2,1,0:T(8,128)(2,1)} %get-tuple-element.9) | copy-start | bytes 12582916
  78.3 2.9 %copy-start.4 = (bf16[1,512,2048]{2,1,0:T(8,128)(2,1)S(1)}, bf16[1,512,2048]{2,1,0:T(8,128)(2,1)}, u32[]{:S(2)}) copy-start(bf16[1,512,2048]{2,1,0:T(8,128)(2,1)} %param.13) | copy-start | bytes 6291460
  139.7 6.4 %copy-start.2 = (bf16[8,128,2048]{2,1,0:T(8,128)(2,1)S(1)}, bf16[8,128,2048]{2,1,0:T(8,128)(2,1)}, u32[]{:S(2)}) copy-start(bf16[8,128,2048]{2,1,0:T(8,128)(2,1)} %get-tuple-element.8) | copy-start | bytes 12582916
  146.1 3.8 %copy-start.7 = (bf16[1024,512]{0,1:T(8,128)(2,1)S(1)}, bf16[1024,512]{0,1:T(8,128)(2,1)}, u32[]{:S(2)}) copy-start(bf16[1024,512]{0,1:T(8,128)(2,1)} %get-tuple-element.14) | copy-start | bytes 3145732
  149.9 2.4 %copy-start.6 = (bf16[1,2048,512]{2,1,0:T(8,128)(2,1)S(1)}, bf16[1,2048,512]{2,1,0:T(8,128)(2,1)}, u32[]{:S(2)}) copy-start(bf16[1,2048,512]{2,1,0:T(8,128)(2,1)} %param.12) | copy-start | bytes 6291460
